TPU v7x, 32 devices: a whole 2x2x4 slice. The times are simulated.
32 devices in a mesh: fs: 8 (over z, core), tp: 4 (over y, x).
Axes of the slice: x: 2, y: 2, z: 4, core: 2. Of those that a mesh axis runs over, the one named last changes fastest.
Arguments:
- tokens: bfloat16 [4096, 4096], P('fs', 'tp'), may hold values from -16 to 16
- norm_gain: float32 [4096], P('fs'), may hold values from 0.1 to 1.9
- gate_train: float32 [4096, 12288], P('fs', 'tp'), may hold values from -6 to 6
- up_train: float32 [4096, 12288], P('fs', 'tp'), may hold values from -6 to 6
Outputs:
- gate_serve: bfloat16 [4096, 12288], P(None, 'tp')
- up_serve: bfloat16 [4096, 12288], P(None, 'tp')
- hidden: bfloat16 [4096, 12288], P('fs', 'tp')
All inputs are finite; a program needn't handle non-finite values.
Results may differ from a plain program's by a relative error of at most 0.0071.
Values may be sent and summed in bfloat16 or wider, within the bound.
A program may use at most 192 MiB of HBM per device.

v0:
```python
import jax
import jax.numpy as jnp
from jax import lax
from jax.sharding import PartitionSpec as P


def body(tokens, norm_gain, gate_train, up_train):
    gain = norm_gain[:, None]
    gate_local = (gate_train * gain).astype(jnp.bfloat16)
    up_local = (up_train * gain).astype(jnp.bfloat16)
    whole = lax.all_gather(tokens, "tp", axis=1, tiled=True)
    values = whole.astype(jnp.float32)
    normed = (values * lax.rsqrt(jnp.mean(values * values, axis=-1, keepdims=True) + 1e-06)).astype(
        jnp.bfloat16
    )
    width = normed.shape[1]
    scale = width ** (-0.5)
    gate_serve, up_serve = (
        lax.all_gather(gate_local, "fs", axis=0, tiled=True),
        lax.all_gather(up_local, "fs", axis=0, tiled=True),
    )
    gate_acc = jnp.dot(normed, gate_serve, preferred_element_type=jnp.float32)
    up_acc = jnp.dot(normed, up_serve, preferred_element_type=jnp.float32)
    gate = gate_acc * scale
    up = up_acc * scale
    hidden = (jax.nn.silu(gate) * up).astype(jnp.bfloat16)
    return (gate_serve, up_serve, hidden)


def solution(mesh):
    in_specs = (P("fs", "tp"), P("fs"), P("fs", "tp"), P("fs", "tp"))
    out_specs = (P(None, "tp"), P(None, "tp"), P("fs", "tp"))
    return jax.shard_map(body, mesh=mesh, in_specs=in_specs, out_specs=out_specs, check_vma=False)
```

profile of v0, /device:TPU:0, one launch (start us, length us, event | category | flops | bytes accessed | tf_op | source)
XLA Modules:
  0.0 569.7 jit_solution(12411793271498854987)
XLA Ops:
  7.2 0.0 all-gather.8.cloned.1.call-start
  7.2 0.7 all-gather.8.cloned.1.call-update
  7.9 0.0 all-gather.4.cloned.1.call-start
  7.9 9.3 %multiply_convert_fusion.1 = (bf16[512,3072]{1,0:T(8,128)(2,1)}, bf16[512,3072]{1,0:T(8,128)(2,1)}) fusion(f32[512,3072]{1,0:T(8,128)} %param.7, f32[512]{0:T(512)} %param.5, f32[512,3072]{1,0:T(8,128)} %param.6), kind=kLoop, calls=%fused_computation.5 | loop fusion | flops 6291456 | bytes 18876416 | tf_op jit(solution)/shard_map/convert_element_type | solution.py:10
  17.2 0.0 all-gather.4.cloned.1.call-update
  17.3 0.0 all-gather.6.cloned.1.call-start
  17.3 0.7 all-gather.6.cloned.1.call-update
  18.0 47.2 %all-gather.8.cloned.1.call-done = bf16[512,4096]{1,0:T(8,128)(2,1)} async-done(((bf16[512,1024]{1,0:T(8,128)(2,1)}), bf16[512,4096]{1,0:T(8,128)(2,1)}) %all-gather.8.cloned.1.call-update) | async-done | bytes 4194320 | tf_op jit(solution)/shard_map/all_gather | solution.py:11
  65.1 3.1 fusion
  68.2 219.0 %all-gather.4.cloned.1.call-done = bf16[4096,3072]{1,0:T(8,128)(2,1)} async-done(((bf16[512,3072]{1,0:T(8,128)(2,1)}), bf16[4096,3072]{1,0:T(8,128)(2,1)}) %all-gather.4.cloned.1.call-update) | async-done | bytes 25165840 | tf_op jit(solution)/shard_map/all_gather | solution.py:19
  287.2 20.6 %fusion.3 = f32[512,3072]{1,0:T(8,128)} fusion(bf16[4096,3072]{1,0:T(8,128)(2,1)} %all-gather.4.cloned.1.call-done, bf16[512,4096]{1,0:T(8,128)(2,1)} %all-gather.8.cloned.1.call-done, f32[512]{0:T(512)S(1)} %add_rsqrt_fusion), kind=kOutput, calls=%fused_computation.7 | convolution fusion | flops 12891193344 | bytes 35653632 | tf_op jit(solution)/shard_map/dot_general | solution.py:22
  307.8 199.7 %all-gather.6.cloned.1.call-done = bf16[4096,3072]{1,0:T(8,128)(2,1)} async-done(((bf16[512,3072]{1,0:T(8,128)(2,1)}), bf16[4096,3072]{1,0:T(8,128)(2,1)}) %all-gather.6.cloned.1.call-update) | async-done | bytes 25165840 | tf_op jit(solution)/shard_map/all_gather | solution.py:20
  507.5 21.8 %multiply_convert_fusion = bf16[512,3072]{1,0:T(8,128)(2,1)} fusion(f32[512,3072]{1,0:T(8,128)} %fusion.3, bf16[4096,3072]{1,0:T(8,128)(2,1)} %all-gather.6.cloned.1.call-done, bf16[512,4096]{1,0:T(8,128)(2,1)} %all-gather.8.cloned.1.call-done, f32[512]{0:T(512)S(1)} %add_rsqrt_fusion), kind=kOutput, calls=%fused_computation.4 | convolution fusion | flops 12903776256 | bytes 38799360 | tf_op jit(solution)/shard_map/dot_general | solution.py:23
  529.4 0.0 copy-start
  529.4 22.0 %copy.9 = bf16[4096,3072]{1,0:T(8,128)(2,1)} copy(bf16[4096,3072]{1,0:T(8,128)(2,1)} %all-gather.4.cloned.1.call-done) | data formatting | bytes 50331648
  551.3 2.9 copy-done
  554.3 8.9 %copy.10 = bf16[4096,3072]{1,0:T(8,128)(2,1)} copy(bf16[4096,3072]{1,0:T(8,128)(2,1)S(1)} %copy-done) | data formatting | bytes 50331648
  (1 shorter events, 0.0 us)
Async XLA Ops:
  7.2 58.0 %all-gather.8.cloned.1.call-start = ((), (), s32[]{:S(2)}) async-start(), calls=%async_computation.2 | async-start | bytes 5242880 | tf_op jit(solution)/shard_map/all_gather | solution.py:11
  7.9 279.3 %all-gather.4.cloned.1.call-start = ((), (), s32[]{:S(2)}) async-start(), calls=%async_computation | async-start | bytes 28311552 | tf_op jit(solution)/shard_map/all_gather | solution.py:19
  17.3 490.3 %all-gather.6.cloned.1.call-start = ((), (), s32[]{:S(2)}) async-start(), calls=%async_computation.1 | async-start | bytes 28311552 | tf_op jit(solution)/shard_map/all_gather | solution.py:20
  529.4 24.9 %copy-start = (bf16[4096,3072]{1,0:T(8,128)(2,1)S(1)}, bf16[4096,3072]{1,0:T(8,128)(2,1)}, u32[]{:S(2)}) copy-start(bf16[4096,3072]{1,0:T(8,128)(2,1)} %all-gather.6.cloned.1.call-done) | copy-start | bytes 75497472
Sparse Core Ops, SparseCore 0:
  9.8 55.2 all-gather.7
  67.4 219.8 all-gather.3
  289.5 218.0 all-gather.5
where the time goes:
time: 570 us
  waiting for transfers between devices  467 us (82%)
  matrix products  42.4 us (7%)
  local copies, waits for them, and re-layouts  33.8 us (6%)
  between operations  13.7 us (2%)
  other arithmetic  12.4 us (2%)
    all_gather x1, waiting for transfers between devices, body(): lax.all_gather(gate_local, 'fs', axis=0, tiled=True)  219 us
    all_gather x1, waiting for transfers between devices, body(): lax.all_gather(up_local, 'fs', axis=0, tiled=True)  200 us
    all_gather x1, waiting for transfers between devices, body(): whole = lax.all_gather(tokens, 'tp', axis=1, tiled=True)  47.2 us
    unnamed x4, local copies, waits for them, and re-layouts  33.8 us
    dot_general x1, matrix products, body(): up_acc = jnp.dot(normed, up_serve, preferred_element_type=jnp.float32)  21.8 us
    dot_general x1, matrix products, body(): gate_acc = jnp.dot(normed, gate_serve, preferred_element_type=jnp.float32)  20.6 us
  transfers between devices with their start and end apart: 3, of which 3 were waited for; matrix products, arithmetic and copies ran while one was open for 6% of the time, Pallas kernels for 0%

commit v1 on v0

v1 whole, which is shorter than its diff:
```python
import functools

import jax
import jax.numpy as jnp
from jax import lax
from jax.experimental import pallas as pl
from jax.experimental.pallas import tpu as pltpu
from jax.sharding import PartitionSpec as P

PIECES = 3


def product(normed_ref, weight_ref, scale):
    return jnp.dot(normed_ref[...], weight_ref[...], preferred_element_type=jnp.float32) * scale


def gate_kernel(scale, normed_ref, weight_ref, *refs):
    serve_ref, gate_ref = refs[-2:]
    serve_ref[...] = weight_ref[...]
    gate_ref[...] = product(normed_ref, weight_ref, scale)


def up_kernel(scale, normed_ref, weight_ref, gate_ref, *refs):
    serve_ref, hidden_ref = refs[-2:]
    serve_ref[...] = weight_ref[...]
    gate = gate_ref[...]
    up = product(normed_ref, weight_ref, scale)
    hidden_ref[...] = (gate / (1.0 + jnp.exp(-gate)) * up).astype(hidden_ref.dtype)


def step(kernel, scale, at, cols, normed, weight, gate, kept):
    depth, width = weight.shape
    toks = normed.shape[0]
    tile = 256 if width % 256 == 0 else width
    first = at * (width // tile)
    here = pl.BlockSpec((depth, tile), lambda i: (0, first + i))
    piece = pl.BlockSpec((depth, tile), lambda i: (0, i))
    local = pl.BlockSpec((toks, tile), lambda i: (0, i))
    there = pl.BlockSpec((toks, tile), lambda i: (0, first + i))
    args, specs = [normed, weight], [pl.BlockSpec((toks, depth), lambda i: (0, 0)), piece]
    serve = jax.ShapeDtypeStruct((depth, cols), weight.dtype)
    if gate is None:
        outs, out_specs = [serve, jax.ShapeDtypeStruct((toks, width), jnp.float32)], [here, local]
    else:
        args.append(gate)
        specs.append(local)
        outs, out_specs = [serve, jax.ShapeDtypeStruct((toks, cols), weight.dtype)], [here, there]
    aliases = {len(args) + k: k for k in range(len(kept))}
    return pl.pallas_call(
        functools.partial(kernel, scale),
        grid=(width // tile,),
        in_specs=specs + [pl.BlockSpec(memory_space=pl.ANY)] * len(kept),
        out_specs=out_specs,
        out_shape=outs,
        input_output_aliases=aliases,
        cost_estimate=pl.CostEstimate(
            flops=2 * toks * depth * width, bytes_accessed=4 * depth * width + 2 * toks * depth, transcendentals=0
        ),
        compiler_params=pltpu.CompilerParams(vmem_limit_bytes=40 * 1024 * 1024),
    )(*args, *kept)


def body(tokens, norm_gain, gate_train, up_train):
    gain = norm_gain[:, None]
    cols = gate_train.shape[1]
    width = cols // PIECES

    def gathered(train, at):
        local = (train[:, at * width : (at + 1) * width] * gain).astype(jnp.bfloat16)
        return lax.all_gather(local, "fs", axis=0, tiled=True)

    tp, mine = lax.axis_size("tp"), lax.axis_index("tp")
    toks, part = tokens.shape
    whole = jnp.zeros((toks, tp * part), tokens.dtype)
    for k in range(tp):
        got = tokens if k == 0 else lax.ppermute(tokens, "tp", [(i, (i + k) % tp) for i in range(tp)])
        whole = lax.dynamic_update_slice(whole, got, (0, lax.rem(mine + tp - k, tp) * part))
    values = whole.astype(jnp.float32)
    normed = (values * lax.rsqrt(jnp.mean(values * values, axis=-1, keepdims=True) + 1e-06)).astype(jnp.bfloat16)
    scale = normed.shape[1] ** (-0.5)

    gates = [gathered(gate_train, at) for at in range(PIECES)]
    ups = [gathered(up_train, at) for at in range(PIECES)]
    gate_kept, up_kept, gate = [], [], []
    for at in range(PIECES):
        served, value = step(gate_kernel, scale, at, cols, normed, gates[at], None, gate_kept)
        gate_kept = [served]
        gate.append(value)
    for at in range(PIECES):
        up_kept = step(up_kernel, scale, at, cols, normed, ups[at], gate[at], up_kept)
    return (gate_kept[0], *up_kept)


def solution(mesh):
    in_specs = (P("fs", "tp"), P("fs"), P("fs", "tp"), P("fs", "tp"))
    out_specs = (P(None, "tp"), P(None, "tp"), P("fs", "tp"))
    return jax.shard_map(body, mesh=mesh, in_specs=in_specs, out_specs=out_specs, check_vma=False)
```

time: 570 us -> 530 us (0.930)
  Pallas kernels: 0 us -> 59.2 us
  waiting for transfers between devices: 467 us -> 420 us
  matrix products: 42.4 us -> 0 us
  local copies, waits for them, and re-layouts: 33.8 us -> 18.3 us
  starting transfers between devices: 0.12 us -> 6.2 us
    all_gather x3 -> x6, waiting for transfers between devices: 466 us -> 375 us  [gathered(): return lax.all_gather(local, 'fs', axis=0, tiled=True)]
    pallas_call x0 -> x6, Pallas kernels: none -> 59.2 us  [step(): pl.pallas_call(functools.partial(kernel, scale), grid=(width // tile,), i...]
    dot_general x2 -> x0, matrix products: 42.4 us -> none  [the longest x1 21.8 us: body(): up_acc = jnp.dot(normed, up_serve, preferred_element_type=jnp.float32)]
    ppermute x0 -> x3, waiting for transfers between devices: none -> 41.8 us  [body(): lax.ppermute(tokens, 'tp', [(i, (i + k) % tp) for i in range(tp)])]
    unnamed x4 -> x18, local copies, waits for them, and re-layouts: 33.8 us -> 16.1 us
    ppermute x0 -> x3, starting transfers between devices: none -> 5.97 us  [body(): lax.ppermute(tokens, 'tp', [(i, (i + k) % tp) for i in range(tp)])]
  transfers between devices with their start and end apart: 3 -> 9, of which waited for: 3 -> 9; matrix products, arithmetic and copies ran while one was open for 6% -> 1% of each run, Pallas kernels for 0% -> 9%
where the time goes in v1:
time: 530 us
  waiting for transfers between devices  420 us (79%)
  Pallas kernels  59.2 us (11%)
  local copies, waits for them, and re-layouts  18.3 us (3%)
  between operations  14.2 us (3%)
  other arithmetic  12.2 us (2%)
  starting transfers between devices  6.2 us (1%)
    all_gather x6, waiting for transfers between devices, gathered(): return lax.all_gather(local, 'fs', axis=0, tiled=True)  375 us
    pallas_call x6, Pallas kernels, step(): pl.pallas_call(functools.partial(kernel, scale), grid=(width // tile,), i...  59.2 us
    ppermute x3, waiting for transfers between devices, body(): lax.ppermute(tokens, 'tp', [(i, (i + k) % tp) for i in range(tp)])  41.8 us
    unnamed x18, local copies, waits for them, and re-layouts  16.1 us
  transfers between devices with their start and end apart: 9, of which 9 were waited for; matrix products, arithmetic and copies ran while one was open for 1% of the time, Pallas kernels for 9%

profile of v1, /device:TPU:0, one launch (start us, length us, event | category | flops | bytes accessed | tf_op | source)
XLA Modules:
  0.0 529.6 jit_solution(6706512204120324010)
XLA Ops:
  7.2 7.8 %multiply_convert_fusion = (bf16[512,1024]{1,0:T(8,128)(2,1)}, bf16[512,1024]{1,0:T(8,128)(2,1)}, bf16[512,1024]{1,0:T(8,128)(2,1)}, bf16[512,1024]{1,0:T(8,128)...) fusion(f32[512,3072]{1,0:T(8,128)} %param.7, f32[512]{0:T(512)} %param.5, f32[512,3072]{1,0:T(8,128)} %param.6), kind=kLoop, calls=%fused_computation.4 | loop fusion | flops 6291456 | bytes 18876416 | tf_op jit(solution)/shard_map/convert_element_type | solution.py:69
  15.1 0.7 all-gather.17.cloned.1.call-update
  15.9 0.7 all-gather.9.cloned.1.call-update
  17.2 0.5 all-gather.15.cloned.1.call-update
  18.3 3.0 collective-permute-start
  21.3 1.5 collective-permute-start.1
  22.8 1.4 collective-permute-start.2
  24.9 21.5 %collective-permute-done = bf16[512,1024]{1,0:T(8,128)(2,1)} collective-permute-done((bf16[512,1024]{1,0:T(8,128)(2,1)S(1)}, bf16[512,1024]{1,0:T(8,128)(2,1)}, u32[]{:S(2)}, u32[]{:S(2)}) %collective-permute-start) | collective-permute-done | bytes 1048608 | tf_op jit(solution)/shard_map/ppermute | solution.py:76
  46.4 1.3 constant_dynamic-update-slice_fusion.2
  47.8 20.1 %collective-permute-done.1 = bf16[512,1024]{1,0:T(8,128)(2,1)S(1)} collective-permute-done((bf16[512,1024]{1,0:T(8,128)(2,1)S(1)}, bf16[512,1024]{1,0:T(8,128)(2,1)S(1)}, u32[]{:S(2)}, u32[]{:S(2)}) %collective-permute-start.1) | collective-permute-done | bytes 1048608 | tf_op jit(solution)/shard_map/ppermute | solution.py:76
  68.3 0.9 fusion
  69.2 3.4 fusion.1.normed_ref
  72.7 27.3 %all-gather.11.cloned.1.call-done.weight_ref = bf16[4096,1024]{1,0:T(8,128)(2,1)} async-done(((bf16[512,1024]{1,0:T(8,128)(2,1)}), bf16[4096,1024]{1,0:T(8,128)(2,1)}) %all-gather.11.cloned.1.call-update) | async-done | bytes 8388624 | tf_op jit(solution)/shard_map/all_gather | solution.py:70
  100.0 2.2 copy-done
  102.2 9.7 %shard_map.67 = (bf16[4096,3072]{1,0:T(8,128)(2,1)}, f32[512,1024]{1,0:T(8,128)S(1)}) custom-call(bf16[512,4096]{1,0:T(8,128)(2,1)S(1)} %copy-done, bf16[4096,1024]{1,0:T(8,128)(2,1)} %all-gather.11.cloned.1.call-done.weight_ref), custom_call_target="tpu_custom_call" | custom-call | flops 4294967296 | bytes 20971520 | tf_op jit(solution)/shard_map/pallas_call | solution.py:49
  111.8 70.9 %all-gather.17.cloned.1.call-done.weight_ref = bf16[4096,1024]{1,0:T(8,128)(2,1)} async-done(((bf16[512,1024]{1,0:T(8,128)(2,1)}), bf16[4096,1024]{1,0:T(8,128)(2,1)}) %all-gather.17.cloned.1.call-update) | async-done | bytes 8388624 | tf_op jit(solution)/shard_map/all_gather | solution.py:70
  182.7 2.2 copy-done.1
  184.9 10.0 %shard_map.70 = (bf16[4096,3072]{1,0:T(8,128)(2,1)}, bf16[512,3072]{1,0:T(8,128)(2,1)}) custom-call(bf16[512,4096]{1,0:T(8,128)(2,1)S(1)} %copy-done.1, bf16[4096,1024]{1,0:T(8,128)(2,1)} %all-gather.17.cloned.1.call-done.weight_ref, f32[512,1024]{1,0:T(8,128)S(1)} %get-tuple-element.20.gate_ref), custom_call_target="tpu_custom_call" | custom-call | flops 4294967296 | bytes 20971520 | tf_op jit(solution)/shard_map/pallas_call | solution.py:49
  194.9 69.9 %all-gather.9.cloned.1.call-done.weight_ref = bf16[4096,1024]{1,0:T(8,128)(2,1)} async-done(((bf16[512,1024]{1,0:T(8,128)(2,1)}), bf16[4096,1024]{1,0:T(8,128)(2,1)}) %all-gather.9.cloned.1.call-update) | async-done | bytes 8388624 | tf_op jit(solution)/shard_map/all_gather | solution.py:70
  264.9 2.2 copy-done.2
  267.0 9.8 %shard_map.68 = (bf16[4096,3072]{1,0:T(8,128)(2,1)}, f32[512,1024]{1,0:T(8,128)S(1)}) custom-call(bf16[512,4096]{1,0:T(8,128)(2,1)S(1)} %copy-done.2, bf16[4096,1024]{1,0:T(8,128)(2,1)} %all-gather.9.cloned.1.call-done.weight_ref, bf16[4096,3072]{1,0:T(8,128)(2,1)} %get-tuple-element.15.refs_0_), custom_call_target="tpu_custom_call", output_to_operand_aliasing={{0}: (2, {})} | custom-call | flops 4294967296 | bytes 20971520 | tf_op jit(solution)/shard_map/pallas_call | solution.py:49
  276.8 1.4 copy-done.6
  278.2 68.7 %all-gather.7.cloned.1.call-done.weight_ref = bf16[4096,1024]{1,0:T(8,128)(2,1)} async-done(((bf16[512,1024]{1,0:T(8,128)(2,1)}), bf16[4096,1024]{1,0:T(8,128)(2,1)}) %all-gather.7.cloned.1.call-update) | async-done | bytes 8388624 | tf_op jit(solution)/shard_map/all_gather | solution.py:70
  346.9 2.2 copy-done.3
  349.1 9.8 %shard_map.69 = (bf16[4096,3072]{1,0:T(8,128)(2,1)}, f32[512,1024]{1,0:T(8,128)S(1)}) custom-call(bf16[512,4096]{1,0:T(8,128)(2,1)S(1)} %copy-done.3, bf16[4096,1024]{1,0:T(8,128)(2,1)} %all-gather.7.cloned.1.call-done.weight_ref, bf16[4096,3072]{1,0:T(8,128)(2,1)} %get-tuple-element.16.refs_0_), custom_call_target="tpu_custom_call", output_to_operand_aliasing={{0}: (2, {})} | custom-call | flops 4294967296 | bytes 20971520 | tf_op jit(solution)/shard_map/pallas_call | solution.py:49
  358.8 70.0 %all-gather.15.cloned.1.call-done.weight_ref = bf16[4096,1024]{1,0:T(8,128)(2,1)} async-done(((bf16[512,1024]{1,0:T(8,128)(2,1)}), bf16[4096,1024]{1,0:T(8,128)(2,1)}) %all-gather.15.cloned.1.call-update) | async-done | bytes 8388624 | tf_op jit(solution)/shard_map/all_gather | solution.py:70
  428.9 2.2 copy-done.4
  431.1 1.6 copy-done.7
  432.6 10.2 %shard_map.71 = (bf16[4096,3072]{1,0:T(8,128)(2,1)}, bf16[512,3072]{1,0:T(8,128)(2,1)}) custom-call(bf16[512,4096]{1,0:T(8,128)(2,1)S(1)} %copy-done.4, bf16[4096,1024]{1,0:T(8,128)(2,1)} %all-gather.15.cloned.1.call-done.weight_ref, f32[512,1024]{1,0:T(8,128)S(1)} %copy-done.7, ...), custom_call_target="tpu_custom_call", output_to_operand_aliasing={{0}: (3, {}), {1}: (4, {})} | custom-call | flops 4294967296 | bytes 20971520 | tf_op jit(solution)/shard_map/pallas_call | solution.py:49
  442.8 68.0 %all-gather.13.cloned.1.call-done.weight_ref = bf16[4096,1024]{1,0:T(8,128)(2,1)} async-done(((bf16[512,1024]{1,0:T(8,128)(2,1)}), bf16[4096,1024]{1,0:T(8,128)(2,1)}) %all-gather.13.cloned.1.call-update) | async-done | bytes 8388624 | tf_op jit(solution)/shard_map/all_gather | solution.py:70
  510.9 2.2 copy-done.5
  513.1 9.7 %shard_map.72 = (bf16[4096,3072]{1,0:T(8,128)(2,1)}, bf16[512,3072]{1,0:T(8,128)(2,1)}) custom-call(bf16[512,4096]{1,0:T(8,128)(2,1)S(1)} %copy-done.5, bf16[4096,1024]{1,0:T(8,128)(2,1)} %all-gather.13.cloned.1.call-done.weight_ref, f32[512,1024]{1,0:T(8,128)S(1)} %get-tuple-element.18.gate_ref, ...), custom_call_target="tpu_custom_call", output_to_operand_aliasing={{0}: (3, {}), {1}: (4, {})} | custom-call | flops 4294967296 | bytes 20971520 | tf_op jit(solution)/shard_map/pallas_call | solution.py:49
  (25 shorter events, 2.3 us)
Async XLA Ops:
  7.2 92.8 %all-gather.11.cloned.1.call-start = ((), (), s32[]{:S(2)}) async-start(), calls=%async_computation.2 | async-start | bytes 9437184 | tf_op jit(solution)/shard_map/all_gather | solution.py:70
  15.0 3.3 copy-start.8
  15.1 167.6 %all-gather.17.cloned.1.call-start = ((), (), s32[]{:S(2)}) async-start(), calls=%async_computation.5 | async-start | bytes 9437184 | tf_op jit(solution)/shard_map/all_gather | solution.py:70
  15.8 249.0 %all-gather.9.cloned.1.call-start = ((), (), s32[]{:S(2)}) async-start(), calls=%async_computation.1 | async-start | bytes 9437184 | tf_op jit(solution)/shard_map/all_gather | solution.py:70
  16.5 330.3 %all-gather.7.cloned.1.call-start = ((), (), s32[]{:S(2)}) async-start(), calls=%async_computation | async-start | bytes 9437184 | tf_op jit(solution)/shard_map/all_gather | solution.py:70
  17.1 411.7 %all-gather.15.cloned.1.call-start = ((), (), s32[]{:S(2)}) async-start(), calls=%async_computation.4 | async-start | bytes 9437184 | tf_op jit(solution)/shard_map/all_gather | solution.py:70
  17.7 493.2 %all-gather.13.cloned.1.call-start = ((), (), s32[]{:S(2)}) async-start(), calls=%async_computation.3 | async-start | bytes 9437184 | tf_op jit(solution)/shard_map/all_gather | solution.py:70
  18.3 28.1 %collective-permute-start = (bf16[512,1024]{1,0:T(8,128)(2,1)S(1)}, bf16[512,1024]{1,0:T(8,128)(2,1)}, u32[]{:S(2)}, u32[]{:S(2)}) collective-permute-start(bf16[512,1024]{1,0:T(8,128)(2,1)S(1)} %copy-done.8), channel_id=1, source_target_pairs={{0,1},{1,2},{2,3},{3,0},{4,5},{5,6},{6,7},{7,4},{8,9},{9,10},{10,1... | collective-permute-start | bytes 3145736 | tf_op jit(solution)/shard_map/ppermute | solution.py:76
  21.3 46.6 %collective-permute-start.1 = (bf16[512,1024]{1,0:T(8,128)(2,1)S(1)}, bf16[512,1024]{1,0:T(8,128)(2,1)S(1)}, u32[]{:S(2)}, u32[]{:S(2)}) collective-permute-start(bf16[512,1024]{1,0:T(8,128)(2,1)S(1)} %copy-done.8), channel_id=1, source_target_pairs={{0,2},{1,3},{2,0},{3,1},{4,6},{5,7},{6,4},{7,5},{8,10},{9,11},{10,... | collective-permute-start | bytes 3145736 | tf_op jit(solution)/shard_map/ppermute | solution.py:76
  22.8 45.4 %collective-permute-start.2 = (bf16[512,1024]{1,0:T(8,128)(2,1)S(1)}, bf16[512,1024]{1,0:T(8,128)(2,1)S(1)}, u32[]{:S(2)}, u32[]{:S(2)}) collective-permute-start(bf16[512,1024]{1,0:T(8,128)(2,1)S(1)} %copy-done.8), channel_id=1, source_target_pairs={{0,3},{1,0},{2,1},{3,2},{4,7},{5,4},{6,5},{7,6},{8,11},{9,8},{10,9... | collective-permute-start | bytes 3145736 | tf_op jit(solution)/shard_map/ppermute | solution.py:76
  100.0 2.2 copy-start
  182.7 2.2 copy-start.1
  264.9 2.2 copy-start.2
  276.8 1.4 copy-start.6
  346.9 2.2 copy-start.3
  428.9 2.2 copy-start.4
  431.1 1.6 copy-start.7
  510.9 2.2 copy-start.5
Sparse Core Ops, SparseCore 0:
  15.2 84.7 all-gather.10
  102.1 80.5 all-gather.16
  184.3 80.5 all-gather.8
  266.3 80.5 all-gather.6
  348.3 80.5 all-gather.14
  430.3 80.5 all-gather.12

commit v2 on v0

v2 whole, which is shorter than its diff:
```python
import functools

import jax
import jax.numpy as jnp
from jax import lax
from jax.experimental import pallas as pl
from jax.experimental.pallas import tpu as pltpu
from jax.sharding import PartitionSpec as P

VMEM = 56 * 1024 * 1024


def call(kernel, grid, in_specs, out_specs, out_shape, flops, moved, aliases=None):
    return pl.pallas_call(
        kernel,
        grid=(grid,),
        in_specs=in_specs,
        out_specs=out_specs,
        out_shape=out_shape,
        input_output_aliases=aliases or {},
        cost_estimate=pl.CostEstimate(flops=flops, bytes_accessed=moved, transcendentals=0),
        compiler_params=pltpu.CompilerParams(vmem_limit_bytes=VMEM),
    )


def fold_kernel(gates, gain_ref, gate_ref, up_ref, out_ref):
    @pl.when(pl.program_id(0) < gates)
    def _():
        out_ref[...] = (gate_ref[...] * gain_ref[...]).astype(out_ref.dtype)

    @pl.when(pl.program_id(0) >= gates)
    def _():
        out_ref[...] = (up_ref[...] * gain_ref[...]).astype(out_ref.dtype)


def product(normed_ref, weight_ref, scale):
    return jnp.dot(normed_ref[...], weight_ref[...], preferred_element_type=jnp.float32) * scale


def gated(gate, up):
    return gate / (1.0 + jnp.exp(-gate)) * up


def both_kernel(scale, normed_ref, gate_ref, up_ref, gate_out, up_out, hidden_ref):
    gate_out[...] = gate_ref[...]
    up_out[...] = up_ref[...]
    gate = product(normed_ref, gate_ref, scale)
    hidden_ref[...] = gated(gate, product(normed_ref, up_ref, scale)).astype(hidden_ref.dtype)


def gate_kernel(scale, normed_ref, weight_ref, _, serve_ref, gate_ref):
    serve_ref[...] = weight_ref[...]
    gate_ref[...] = product(normed_ref, weight_ref, scale)


def up_kernel(scale, normed_ref, weight_ref, gate_ref, _, __, serve_ref, hidden_ref):
    serve_ref[...] = weight_ref[...]
    hidden_ref[...] = gated(gate_ref[...], product(normed_ref, weight_ref, scale)).astype(hidden_ref.dtype)


def body(tokens, norm_gain, gate_train, up_train):
    gain = norm_gain[:, None]
    rows, cols = gate_train.shape
    last = max(cols // 4 // 128, 1) * 128
    while cols % last:
        last -= 128
    first = cols - last

    gates, tiles = cols // last, (cols + first) // last
    block = lambda index: pl.BlockSpec((rows, last), index)
    local = call(
        functools.partial(fold_kernel, gates),
        tiles,
        [
            pl.BlockSpec((rows, 1), lambda i: (0, 0)),
            block(lambda i: (0, jnp.minimum(i, gates - 1))),
            block(lambda i: (0, jnp.maximum(i - gates, 0))),
        ],
        block(lambda i: (0, i)),
        jax.ShapeDtypeStruct((rows, cols + first), jnp.bfloat16),
        2 * rows * (cols + first),
        6 * rows * (cols + first),
    )(gain, gate_train, up_train)
    main = lax.all_gather(local, "fs", axis=0, tiled=True)
    rest = lax.all_gather((up_train[:, first:] * gain).astype(jnp.bfloat16), "fs", axis=0, tiled=True)

    tp, mine = lax.axis_size("tp"), lax.axis_index("tp")
    toks, part = tokens.shape
    whole = jnp.zeros((toks, tp * part), tokens.dtype)
    for k in range(tp):
        got = tokens if k == 0 else lax.ppermute(tokens, "tp", [(i, (i + k) % tp) for i in range(tp)])
        whole = lax.dynamic_update_slice(whole, got, (0, lax.rem(mine + tp - k, tp) * part))
    values = whole.astype(jnp.float32)
    normed = (values * lax.rsqrt(jnp.mean(values * values, axis=-1, keepdims=True) + 1e-06)).astype(jnp.bfloat16)
    depth = normed.shape[1]
    scale = depth ** (-0.5)

    tile = 256 if last % 256 == 0 else 128
    n_all, n_first, n_last = cols // tile, first // tile, last // tile
    resident = pl.BlockSpec((toks, depth), lambda i: (0, 0))
    weight = lambda at: pl.BlockSpec((depth, tile), lambda i: (0, at + i))
    units = lambda at: pl.BlockSpec((toks, tile), lambda i: (0, at + i))
    anywhere = pl.BlockSpec(memory_space=pl.ANY)
    serve = jax.ShapeDtypeStruct((depth, cols), jnp.bfloat16)
    hidden = jax.ShapeDtypeStruct((toks, cols), jnp.bfloat16)
    flops, moved = 2 * toks * depth * tile, 4 * depth * tile

    gate_serve, up_serve, out = call(
        functools.partial(both_kernel, scale),
        n_first,
        [resident, weight(0), weight(n_all)],
        [weight(0), weight(0), units(0)],
        [serve, serve, hidden],
        2 * n_first * flops,
        2 * n_first * moved,
    )(normed, main, main)
    gate_serve, gate = call(
        functools.partial(gate_kernel, scale),
        n_last,
        [resident, weight(n_first), anywhere],
        [weight(n_first), units(0)],
        [serve, jax.ShapeDtypeStruct((toks, last), jnp.float32)],
        n_last * flops,
        n_last * moved,
        {2: 0},
    )(normed, main, gate_serve)
    up_serve, out = call(
        functools.partial(up_kernel, scale),
        n_last,
        [resident, weight(0), units(0), anywhere, anywhere],
        [weight(n_first), units(n_first)],
        [serve, hidden],
        n_last * flops,
        n_last * moved,
        {3: 0, 4: 1},
    )(normed, rest, gate, up_serve, out)
    return gate_serve, up_serve, out


def solution(mesh):
    in_specs = (P("fs", "tp"), P("fs"), P("fs", "tp"), P("fs", "tp"))
    out_specs = (P(None, "tp"), P(None, "tp"), P("fs", "tp"))
    return jax.shard_map(body, mesh=mesh, in_specs=in_specs, out_specs=out_specs, check_vma=False)
```

time: 570 us -> 478 us (0.84)
  waiting for transfers between devices: 467 us -> 381 us
  Pallas kernels: 0 us -> 66.2 us
  matrix products: 42.4 us -> 0 us
  local copies, waits for them, and re-layouts: 33.8 us -> 4.33 us
  starting transfers between devices: 0.12 us -> 6.05 us
    all_gather x3 -> x2, waiting for transfers between devices: 466 us -> 339 us  [the longest x1 321 us: body(): main = lax.all_gather(local, 'fs', axis=0, tiled=True)]
    pallas_call x0 -> x4, Pallas kernels: none -> 66.2 us  [the longest x1 37.2 us: body(): call(functools.partial(both_kernel, scale), n_first, [resident, weight(0)...]
    dot_general x2 -> x0, matrix products: 42.4 us -> none  [the longest x1 21.8 us: body(): up_acc = jnp.dot(normed, up_serve, preferred_element_type=jnp.float32)]
    ppermute x0 -> x3, waiting for transfers between devices: none -> 41.8 us  [body(): lax.ppermute(tokens, 'tp', [(i, (i + k) % tp) for i in range(tp)])]
    unnamed x4, local copies, waits for them, and re-layouts: 33.8 us -> 0.61 us
    ppermute x0 -> x3, starting transfers between devices: none -> 5.97 us  [body(): lax.ppermute(tokens, 'tp', [(i, (i + k) % tp) for i in range(tp)])]
  transfers between devices with their start and end apart: 3 -> 5, of which waited for: 3 -> 5; matrix products, arithmetic and copies ran while one was open for 6% -> 2% of each run, Pallas kernels for 0% -> 10%
where the time goes in v2:
time: 478 us
  waiting for transfers between devices  381 us (80%)
  Pallas kernels  66.2 us (14%)
  between operations  14.1 us (3%)
  other arithmetic  6.79 us (1%)
  starting transfers between devices  6.05 us (1%)
    all_gather x1, waiting for transfers between devices, body(): main = lax.all_gather(local, 'fs', axis=0, tiled=True)  321 us
    ppermute x3, waiting for transfers between devices, body(): lax.ppermute(tokens, 'tp', [(i, (i + k) % tp) for i in range(tp)])  41.8 us
    pallas_call x1, Pallas kernels, body(): call(functools.partial(both_kernel, scale), n_first, [resident, weight(0)...  37.2 us
    all_gather x1, waiting for transfers between devices, body(): lax.all_gather((up_train[:, first:] * gain).astype(jnp.bfloat16), 'fs', a...  17.4 us
    pallas_call x1, Pallas kernels, body(): call(functools.partial(up_kernel, scale), n_last, [resident, weight(0), u...  10.4 us
    pallas_call x1, Pallas kernels, body(): call(functools.partial(gate_kernel, scale), n_last, [resident, weight(n_f...  10.2 us
  transfers between devices with their start and end apart: 5, of which 5 were waited for; matrix products, arithmetic and copies ran while one was open for 2% of the time, Pallas kernels for 10%

profile of v2, /device:TPU:0, one launch (start us, length us, event | category | flops | bytes accessed | tf_op | source)
XLA Modules:
  0.0 478.1 jit_solution(13997649820583347206)
XLA Ops:
  7.2 0.0 all-gather.3.cloned.1.call-start
  7.2 1.5 copy.10.gain_ref
  8.7 8.4 %shard_map.67 = bf16[512,5376]{1,0:T(8,128)(2,1)} custom-call(f32[512,1]{1,0:T(8,128)} %copy.10.gain_ref, f32[512,3072]{1,0:T(8,128)} %gate_ref.1, f32[512,3072]{1,0:T(8,128)} %up_ref.1), custom_call_target="tpu_custom_call" | custom-call | flops 5505024 | bytes 16515072 | tf_op jit(solution)/shard_map/pallas_call | solution.py:71
  17.2 0.0 copy-start.1
  17.2 0.0 copy-start
  17.2 0.0 all-gather.3.cloned.1.call-update
  17.2 0.0 all-gather.5.cloned.1.call-start
  17.2 0.6 copy-done.1
  17.8 2.4 multiply_convert_fusion
  20.3 0.0 all-gather.5.cloned.1.call-update
  20.3 0.0 copy-done
  20.3 3.0 collective-permute-start
  23.3 1.5 collective-permute-start.1
  24.9 1.4 collective-permute-start.2
  26.3 0.5 broadcast_in_dim.7
  26.8 0.1 constant_dynamic-update-slice_fusion.3
  26.9 21.5 %collective-permute-done = bf16[512,1024]{1,0:T(8,128)(2,1)} collective-permute-done((bf16[512,1024]{1,0:T(8,128)(2,1)S(1)}, bf16[512,1024]{1,0:T(8,128)(2,1)}, u32[]{:S(2)}, u32[]{:S(2)}) %collective-permute-start) | collective-permute-done | bytes 1048608 | tf_op jit(solution)/shard_map/ppermute | solution.py:91
  48.5 1.3 constant_dynamic-update-slice_fusion.2
  49.8 20.1 %collective-permute-done.1 = bf16[512,1024]{1,0:T(8,128)(2,1)S(1)} collective-permute-done((bf16[512,1024]{1,0:T(8,128)(2,1)S(1)}, bf16[512,1024]{1,0:T(8,128)(2,1)S(1)}, u32[]{:S(2)}, u32[]{:S(2)}) %collective-permute-start.1) | collective-permute-done | bytes 1048608 | tf_op jit(solution)/shard_map/ppermute | solution.py:91
  69.9 0.1 constant_dynamic-update-slice_fusion.1
  70.0 0.2 collective-permute-done.2
  70.2 0.1 constant_dynamic-update-slice_fusion
  70.3 0.9 fusion
  71.2 3.5 fusion.1.normed_ref
  74.7 321.4 %all-gather.3.cloned.1.call-done.gate_ref.up_ref.weight_ref = bf16[4096,5376]{1,0:T(8,128)(2,1)} async-done(((bf16[512,5376]{1,0:T(8,128)(2,1)}), bf16[4096,5376]{1,0:T(8,128)(2,1)}) %all-gather.3.cloned.1.call-update) | async-done | bytes 44040208 | tf_op jit(solution)/shard_map/all_gather | solution.py:84
  396.1 37.2 %shard_map.68 = (bf16[4096,3072]{1,0:T(8,128)(2,1)}, bf16[4096,3072]{1,0:T(8,128)(2,1)}, bf16[512,3072]{1,0:T(8,128)(2,1)}) custom-call(bf16[512,4096]{1,0:T(8,128)(2,1)} %fusion.1.normed_ref, bf16[4096,5376]{1,0:T(8,128)(2,1)} %all-gather.3.cloned.1.call-done.gate_ref.up_ref.weight_ref, ...), custom_call_target="tpu_custom_call" | custom-call | flops 19327352832 | bytes 75497472 | tf_op jit(solution)/shard_map/pallas_call | solution.py:108
  433.3 10.2 %shard_map.69 = (bf16[4096,3072]{1,0:T(8,128)(2,1)}, f32[512,768]{1,0:T(8,128)}) custom-call(bf16[512,4096]{1,0:T(8,128)(2,1)} %fusion.1.normed_ref, bf16[4096,5376]{1,0:T(8,128)(2,1)} %all-gather.3.cloned.1.call-done.gate_ref.up_ref.weight_ref, bf16[4096,3072]{1,0:T(8,128)(2,1)} %get-tuple-element.10._), custom_call_target="tpu_custom_call", output_to_operand_aliasing={{0}: (2, {})} | custom-call | flops 3221225472 | bytes 12582912 | tf_op jit(solution)/shard_map/pallas_call | solution.py:117
  443.5 17.4 %all-gather.5.cloned.1.call-done.weight_ref = bf16[4096,768]{1,0:T(8,128)(2,1)} async-done(((bf16[512,768]{1,0:T(8,128)(2,1)}), bf16[4096,768]{1,0:T(8,128)(2,1)}) %all-gather.5.cloned.1.call-update) | async-done | bytes 6291472 | tf_op jit(solution)/shard_map/all_gather | solution.py:85
  460.9 10.4 %shard_map.70 = (bf16[4096,3072]{1,0:T(8,128)(2,1)}, bf16[512,3072]{1,0:T(8,128)(2,1)}) custom-call(bf16[512,4096]{1,0:T(8,128)(2,1)} %fusion.1.normed_ref, bf16[4096,768]{1,0:T(8,128)(2,1)} %all-gather.5.cloned.1.call-done.weight_ref, f32[512,768]{1,0:T(8,128)} %get-tuple-element.12.gate_ref, ...), custom_call_target="tpu_custom_call", output_to_operand_aliasing={{0}: (3, {}), {1}: (4, {})} | custom-call | flops 3221225472 | bytes 12582912 | tf_op jit(solution)/shard_map/pallas_call | solution.py:127
  (1 shorter events, 0.0 us)
Async XLA Ops:
  7.2 388.9 %all-gather.3.cloned.1.call-start = ((), (), s32[]{:S(2)}) async-start(), calls=%async_computation | async-start | bytes 49545216 | tf_op jit(solution)/shard_map/all_gather | solution.py:84
  17.2 0.7 copy-start.1
  17.2 3.1 copy-start
  17.2 443.7 %all-gather.5.cloned.1.call-start = ((), (), s32[]{:S(2)}) async-start(), calls=%async_computation.1 | async-start | bytes 7077888 | tf_op jit(solution)/shard_map/all_gather | solution.py:85
  20.3 28.1 %collective-permute-start = (bf16[512,1024]{1,0:T(8,128)(2,1)S(1)}, bf16[512,1024]{1,0:T(8,128)(2,1)}, u32[]{:S(2)}, u32[]{:S(2)}) collective-permute-start(bf16[512,1024]{1,0:T(8,128)(2,1)S(1)} %copy-done), channel_id=1, source_target_pairs={{0,1},{1,2},{2,3},{3,0},{4,5},{5,6},{6,7},{7,4},{8,9},{9,10},{10,1... | collective-permute-start | bytes 3145736 | tf_op jit(solution)/shard_map/ppermute | solution.py:91
  23.3 46.6 %collective-permute-start.1 = (bf16[512,1024]{1,0:T(8,128)(2,1)S(1)}, bf16[512,1024]{1,0:T(8,128)(2,1)S(1)}, u32[]{:S(2)}, u32[]{:S(2)}) collective-permute-start(bf16[512,1024]{1,0:T(8,128)(2,1)S(1)} %copy-done), channel_id=1, source_target_pairs={{0,2},{1,3},{2,0},{3,1},{4,6},{5,7},{6,4},{7,5},{8,10},{9,11},{10,... | collective-permute-start | bytes 3145736 | tf_op jit(solution)/shard_map/ppermute | solution.py:91
  24.9 45.4 %collective-permute-start.2 = (bf16[512,1024]{1,0:T(8,128)(2,1)S(1)}, bf16[512,1024]{1,0:T(8,128)(2,1)S(1)}, u32[]{:S(2)}, u32[]{:S(2)}) collective-permute-start(bf16[512,1024]{1,0:T(8,128)(2,1)S(1)} %copy-done), channel_id=1, source_target_pairs={{0,3},{1,0},{2,1},{3,2},{4,7},{5,4},{6,5},{7,6},{8,11},{9,8},{10,9... | collective-permute-start | bytes 3145736 | tf_op jit(solution)/shard_map/ppermute | solution.py:91
Sparse Core Ops, SparseCore 0:
  17.3 378.7 all-gather.2
  397.7 63.1 all-gather.4

commit v3 on v2

--- a/solution.py
+++ b/solution.py
@@ -8,6 +8,8 @@
 from jax.sharding import PartitionSpec as P
 
 VMEM = 56 * 1024 * 1024
+CORES = 2
+PIECES = 4
 
 
 def call(kernel, grid, in_specs, out_specs, out_shape, flops, moved, aliases=None):
@@ -31,6 +33,138 @@
     @pl.when(pl.program_id(0) >= gates)
     def _():
         out_ref[...] = (up_ref[...] * gain_ref[...]).astype(out_ref.dtype)
+
+
+def line_kernel(chips, tp, local_ref, tok_ref, out_ref, all_ref, own_sem, tok_send, tok_recv, send, recv, pass_send, pass_recv):
+    me = lax.axis_index("fs")
+    z, core = me // CORES, me % CORES
+    piece = local_ref.shape[0] // PIECES
+    up, down = lax.rem(z + 1, chips), lax.rem(z + chips - 1, chips)
+    peer = z * CORES + (1 - core)
+
+    barrier = pltpu.get_barrier_semaphore()
+    for device in (up * CORES + core, down * CORES + core, peer):
+        pl.semaphore_signal(barrier, inc=1, device_id={"fs": device}, device_id_type=pl.DeviceIdType.MESH)
+    mine = lax.axis_index("tp")
+    for k in range(1, tp):
+        pl.semaphore_signal(
+            barrier, inc=1, device_id={"tp": lax.rem(mine + k, tp)}, device_id_type=pl.DeviceIdType.MESH
+        )
+    pl.semaphore_wait(barrier, 3 + tp - 1)
+
+    part = tok_ref.shape[1]
+
+    def features(k):
+        return pltpu.make_async_remote_copy(
+            src_ref=tok_ref, dst_ref=all_ref.at[:, pl.ds(pl.multiple_of(mine * part, 128), part)],
+            send_sem=tok_send.at[k], recv_sem=tok_recv.at[k],
+            device_id={"tp": lax.rem(mine + k, tp)}, device_id_type=pl.DeviceIdType.MESH,
+        )
+
+    def rows(q):
+        return pl.ds(q * piece, piece)
+
+    def move(src, block, q, device, send_sem, recv_sem):
+        return pltpu.make_async_remote_copy(
+            src_ref=src, dst_ref=out_ref.at[block, rows(q)], send_sem=send_sem, recv_sem=recv_sem,
+            device_id={"fs": device}, device_id_type=pl.DeviceIdType.MESH,
+        )
+
+    def held(way, p):
+        chip = z - p if way == 0 else z + p
+        there = chip >= 0 if way == 0 else chip < chips
+        return lax.clamp(0, chip, chips - 1), there
+
+    def hop(way, p, q, src):
+        chip, there = held(way, p)
+        onward = there & (z < chips - 1 if way == 0 else z > 0)
+        block = chip * CORES + core
+        src = out_ref.at[block, rows(q)] if src is None else src
+        device = (up if way == 0 else down) * CORES + core
+        return onward, move(src, block, q, device, send.at[way, p, q], recv.at[way, p, q])
+
+    def arrival(way, p, q):
+        chip, there = held(way, p + 1)
+        here = out_ref.at[chip * CORES + core, rows(q)]
+        return there, move(here, chip * CORES + core, q, peer, send.at[way, p, q], recv.at[way, p, q])
+
+    def passing(way, p, q, src, mine):
+        chip, there = held(way, p)
+        block = chip * CORES + (core if mine else 1 - core)
+        src = out_ref.at[block, rows(q)] if src is None else src
+        return there, move(src, block, q, peer, pass_send.at[way, p, q], pass_recv.at[way, p, q])
+
+    own = pltpu.make_async_copy(local_ref, out_ref.at[me], own_sem)
+    for q in range(PIECES):
+        for way in range(2):
+            onward, copy = hop(way, 0, q, local_ref.at[rows(q)])
+            pl.when(onward)(copy.start)
+    for q in range(PIECES):
+        passing(0, 0, q, local_ref.at[rows(q)], True)[1].start()
+    own.start()
+    for k in range(1, tp):
+        features(k).start()
+    own_features = pltpu.make_async_copy(
+        tok_ref, all_ref.at[:, pl.ds(pl.multiple_of(mine * part, 128), part)], tok_send.at[0]
+    )
+    own_features.start()
+
+    @pl.loop(1, chips)
+    def _(p):
+        for q in range(PIECES):
+            for way in range(2):
+                there, copy = arrival(way, p - 1, q)
+                pl.when(there)(copy.wait_recv)
+                onward, copy = hop(way, p, q, None)
+                pl.when(onward)(copy.start)
+                there, copy = passing(way, p, q, None, True)
+                pl.when(there)(copy.start)
+
+    own.wait()
+    own_features.wait()
+    for k in range(1, tp):
+        features(k).wait()
+    for q in range(PIECES):
+        copy = passing(0, 0, q, local_ref.at[rows(q)], True)[1]
+        copy.wait_send()
+        passing(0, 0, q, None, False)[1].wait_recv()
+        for way in range(2):
+            onward, copy = hop(way, 0, q, local_ref.at[rows(q)])
+            pl.when(onward)(copy.wait_send)
+
+    @pl.loop(1, chips)
+    def _(p):
+        for q in range(PIECES):
+            for way in range(2):
+                onward, copy = hop(way, p, q, None)
+                pl.when(onward)(copy.wait_send)
+                there, copy = passing(way, p, q, None, True)
+                pl.when(there)(copy.wait_send)
+                there, copy = passing(way, p, q, None, False)
+                pl.when(there)(copy.wait_recv)
+
+
+def line_gather(local, tokens):
+    tp = lax.axis_size("tp")
+    toks, part = tokens.shape
+    fs = lax.axis_size("fs")
+    chips = fs // CORES
+    (rows, width) = local.shape
+    sems = pltpu.SemaphoreType.DMA((2, chips, PIECES))
+    tok_sems = pltpu.SemaphoreType.DMA((tp,))
+    out, whole = pl.pallas_call(
+        functools.partial(line_kernel, chips, tp),
+        in_specs=[pl.BlockSpec(memory_space=pl.ANY)] * 2,
+        out_specs=[pl.BlockSpec(memory_space=pl.ANY)] * 2,
+        out_shape=[
+            jax.ShapeDtypeStruct((fs, rows, width), local.dtype),
+            jax.ShapeDtypeStruct((toks, tp * part), tokens.dtype),
+        ],
+        scratch_shapes=[pltpu.SemaphoreType.DMA, tok_sems, tok_sems, sems, sems, sems, sems],
+        cost_estimate=pl.CostEstimate(flops=2 * 10**11, bytes_accessed=2 * fs * rows * width, transcendentals=0),
+        compiler_params=pltpu.CompilerParams(collective_id=0, has_side_effects=True, vmem_limit_bytes=VMEM),
+    )(local, tokens)
+    return out.reshape(fs * rows, width), whole
 
 
 def product(normed_ref, weight_ref, scale):
@@ -81,15 +215,11 @@
         2 * rows * (cols + first),
         6 * rows * (cols + first),
     )(gain, gate_train, up_train)
-    main = lax.all_gather(local, "fs", axis=0, tiled=True)
-    rest = lax.all_gather((up_train[:, first:] * gain).astype(jnp.bfloat16), "fs", axis=0, tiled=True)
-
-    tp, mine = lax.axis_size("tp"), lax.axis_index("tp")
-    toks, part = tokens.shape
-    whole = jnp.zeros((toks, tp * part), tokens.dtype)
-    for k in range(tp):
-        got = tokens if k == 0 else lax.ppermute(tokens, "tp", [(i, (i + k) % tp) for i in range(tp)])
-        whole = lax.dynamic_update_slice(whole, got, (0, lax.rem(mine + tp - k, tp) * part))
+    (main, whole), rest = lax.optimization_barrier(
+        (line_gather(local, tokens), (up_train[:, first:] * gain).astype(jnp.bfloat16))
+    )
+    rest = lax.all_gather(rest, "fs", axis=0, tiled=True)
+    toks = tokens.shape[0]
     values = whole.astype(jnp.float32)
     normed = (values * lax.rsqrt(jnp.mean(values * values, axis=-1, keepdims=True) + 1e-06)).astype(jnp.bfloat16)
     depth = normed.shape[1]

time: 478 us -> 466 us (0.975)
  waiting for transfers between devices: 381 us -> 10.1 us
  Pallas kernels: 66.2 us -> 430 us
  starting transfers between devices: 6.05 us -> 0.04 us
    pallas_call x0 -> x1, Pallas kernels: none -> 364 us  [line_gather(): pl.pallas_call(functools.partial(line_kernel, chips, tp), in_specs=[pl.Bl...]
    all_gather x2 -> x1, waiting for transfers between devices: 339 us -> 10.1 us  [body(): rest = lax.all_gather(rest, 'fs', axis=0, tiled=True)]
    ppermute x3 -> x0, waiting for transfers between devices: 41.8 us -> none  [body(): lax.ppermute(tokens, 'tp', [(i, (i + k) % tp) for i in range(tp)])]
    ppermute x3 -> x0, starting transfers between devices: 5.97 us -> none  [body(): lax.ppermute(tokens, 'tp', [(i, (i + k) % tp) for i in range(tp)])]
  transfers between devices with their start and end apart: 5 -> 1, of which waited for: 5 -> 1; matrix products, arithmetic and copies ran while one was open for 2% -> 1% of each run, Pallas kernels for 10% -> 10%
where the time goes in v3:
time: 466 us; the launch traced here: 465 us
  Pallas kernels  430 us (92%)
  between operations  14 us (3%)
  waiting for transfers between devices  10.1 us (2%)
  other arithmetic  9.11 us (2%)
    pallas_call x1, Pallas kernels, line_gather(): pl.pallas_call(functools.partial(line_kernel, chips, tp), in_specs=[pl.Bl...  364 us
    pallas_call x1, Pallas kernels, body(): call(functools.partial(both_kernel, scale), n_first, [resident, weight(0)...  36.9 us
    pallas_call x1, Pallas kernels, body(): call(functools.partial(up_kernel, scale), n_last, [resident, weight(0), u...  10.4 us
    pallas_call x1, Pallas kernels, body(): call(functools.partial(gate_kernel, scale), n_last, [resident, weight(n_f...  10.2 us
    all_gather x1, waiting for transfers between devices, body(): rest = lax.all_gather(rest, 'fs', axis=0, tiled=True)  10.1 us
  transfers between devices with their start and end apart: 1, of which 1 were waited for; matrix products, arithmetic and copies ran while one was open for 1% of the time, Pallas kernels for 10%

profile of v3, /device:TPU:0, one launch (start us, length us, event | category | flops | bytes accessed | tf_op | source)
XLA Modules:
  0.0 465.4 jit_solution(3773278960932872376)
XLA Ops:
  7.2 0.0 all-gather.2.cloned.1.call-start
  7.2 1.5 copy.10.gain_ref
  8.7 2.4 multiply_convert_fusion
  11.2 8.4 %shard_map.67.local_ref = bf16[512,5376]{1,0:T(8,128)(2,1)} custom-call(f32[512,1]{1,0:T(8,128)} %copy.10.gain_ref, f32[512,3072]{1,0:T(8,128)} %gate_ref.1, f32[512,3072]{1,0:T(8,128)} %up_ref.1), custom_call_target="tpu_custom_call" | custom-call | flops 5505024 | bytes 16515072 | tf_op jit(solution)/shard_map/pallas_call | solution.py:205
  19.6 364.5 %shard_map.68 = (bf16[8,512,5376]{2,1,0:T(8,128)(2,1)}, bf16[512,4096]{1,0:T(8,128)(2,1)}) custom-call(bf16[512,5376]{1,0:T(8,128)(2,1)} %shard_map.67.local_ref, bf16[512,1024]{1,0:T(8,128)(2,1)} %tok_ref.1), custom_call_target="tpu_custom_call" | custom-call | flops 199999995904 | bytes 44040192 | tf_op jit(solution)/shard_map/pallas_call | solution.py:155
  384.1 0.0 all-gather.2.cloned.1.call-update
  384.1 0.0 copy-start
  384.1 3.2 fusion
  387.4 0.2 copy-done
  387.6 3.4 fusion.1.normed_ref
  391.0 36.9 %shard_map.69 = (bf16[4096,3072]{1,0:T(8,128)(2,1)}, bf16[4096,3072]{1,0:T(8,128)(2,1)}, bf16[512,3072]{1,0:T(8,128)(2,1)}) custom-call(bf16[512,4096]{1,0:T(8,128)(2,1)} %fusion.1.normed_ref, bf16[4096,5376]{1,0:T(8,128)(2,1)} %bitcast.2, bf16[4096,5376]{1,0:T(8,128)(2,1)} %bitcast.3), custom_call_target="tpu_custom_call" | custom-call | flops 19327352832 | bytes 75497472 | tf_op jit(solution)/shard_map/pallas_call | solution.py:238
  427.9 10.2 %shard_map.70 = (bf16[4096,3072]{1,0:T(8,128)(2,1)}, f32[512,768]{1,0:T(8,128)}) custom-call(bf16[512,4096]{1,0:T(8,128)(2,1)} %fusion.1.normed_ref, bf16[4096,5376]{1,0:T(8,128)(2,1)} %bitcast.4, bf16[4096,3072]{1,0:T(8,128)(2,1)} %get-tuple-element.19._), custom_call_target="tpu_custom_call", output_to_operand_aliasing={{0}: (2, {})} | custom-call | flops 3221225472 | bytes 12582912 | tf_op jit(solution)/shard_map/pallas_call | solution.py:247
  438.1 10.1 %all-gather.2.cloned.1.call-done.weight_ref = bf16[4096,768]{1,0:T(8,128)(2,1)} async-done(((bf16[512,768]{1,0:T(8,128)(2,1)}), bf16[4096,768]{1,0:T(8,128)(2,1)}) %all-gather.2.cloned.1.call-update) | async-done | bytes 6291472 | tf_op jit(solution)/shard_map/all_gather | solution.py:221
  448.2 10.4 %shard_map.71 = (bf16[4096,3072]{1,0:T(8,128)(2,1)}, bf16[512,3072]{1,0:T(8,128)(2,1)}) custom-call(bf16[512,4096]{1,0:T(8,128)(2,1)} %fusion.1.normed_ref, bf16[4096,768]{1,0:T(8,128)(2,1)} %all-gather.2.cloned.1.call-done.weight_ref, f32[512,768]{1,0:T(8,128)} %get-tuple-element.22.gate_ref, ...), custom_call_target="tpu_custom_call", output_to_operand_aliasing={{0}: (3, {}), {1}: (4, {})} | custom-call | flops 3221225472 | bytes 12582912 | tf_op jit(solution)/shard_map/pallas_call | solution.py:257
  (1 shorter events, 0.0 us)
Async XLA Ops:
  7.2 441.0 %all-gather.2.cloned.1.call-start = ((), (), s32[]{:S(2)}) async-start(), calls=%async_computation | async-start | bytes 7077888 | tf_op jit(solution)/shard_map/all_gather | solution.py:221
  384.1 3.5 copy-start
Sparse Core Ops, SparseCore 0:
  384.2 63.9 all-gather.1
